TPU v7x, 32 devices: a whole 2x2x4 slice. The times are simulated.
32 devices in a mesh: fs: 4 (over z), rep: 4 (over y, x), tp: 2 (over core).
Axes of the slice: x: 2, y: 2, z: 4, core: 2. Of those that a mesh axis runs over, the one named last changes fastest.
Arguments:
- input_act: bfloat16 [12288, 2048], P(('fs', 'rep')), may hold values from -6 to 6
- query_cot: bfloat16 [12288, 1024], P(('fs', 'rep'), 'tp'), may hold values from -6 to 6
- out_cot: bfloat16 [12288, 2048], P(('fs', 'rep')), may hold values from -6 to 6
- attn_out: bfloat16 [12288, 1024], P(('fs', 'rep'), 'tp'), may hold values from -6 to 6
- query_w: float32 [2048, 1024], P('fs', 'tp'), may hold values from -0.125 to 0.125
- out_w: float32 [1024, 2048], P('tp', 'fs'), may hold values from -0.1875 to 0.1875
- query_factor: bfloat16 [2048, 512], P('fs'), may hold values from -0.125 to 0.125
- out_factor: bfloat16 [2048, 512], P('fs'), may hold values from -0.125 to 0.125
- first_q: float32 [512, 1024], P('fs', 'tp'), may hold values from -6 to 6
- second_q: float32 [512, 1024], P('fs', 'tp'), may hold values from 0.075 to 120
- first_o: float32 [512, 1024], P('fs', 'tp'), may hold values from -6 to 6
- second_o: float32 [512, 1024], P('fs', 'tp'), may hold values from 0.075 to 120
Outputs:
- new_query_w: float32 [2048, 1024], P('fs', 'tp')
- new_out_w: float32 [1024, 2048], P('tp', 'fs')
- query_step: float32 [2048, 1024], P('fs', 'tp')
- out_step: float32 [1024, 2048], P('tp', 'fs')
- new_first_q: float32 [512, 1024], P('fs', 'tp')
- new_second_q: float32 [512, 1024], P('fs', 'tp')
- new_first_o: float32 [512, 1024], P('fs', 'tp')
- new_second_o: float32 [512, 1024], P('fs', 'tp')
- query_copy: bfloat16 [2048, 1024], P(None, 'tp')
- out_copy: bfloat16 [1024, 2048], P('tp')
All inputs are finite; a program needn't handle non-finite values.
Results may differ from a plain program's by a relative error of at most 0.0085.
Values may be sent and summed in bfloat16 or wider, within the bound.
A program may use at most 64 MiB of HBM per device.

v0:
```python
import math
import jax
import jax.numpy as jnp
from jax import lax
from jax.sharding import PartitionSpec as P

RANK = 512
HQ = 1024


def contract_rows(left_side, right_side):
    return lax.dot_general(
        left_side, right_side, (((0,), (0,)), ((), ())), preferred_element_type=jnp.float32
    )


def contract_exact(left_side, right_side):
    return lax.dot_general(
        left_side.astype(jnp.float32),
        right_side,
        (((0,), (0,)), ((), ())),
        precision=lax.Precision.HIGHEST,
        preferred_element_type=jnp.float32,
    )


def exact_dot(left_side, right_side):
    return jnp.dot(
        left_side, right_side, precision=lax.Precision.HIGHEST, preferred_element_type=jnp.float32
    )


def body(
    input_act,
    query_cot,
    out_cot,
    attn_out,
    query_w,
    out_w,
    query_factor,
    out_factor,
    first_q,
    second_q,
    first_o,
    second_o,
):
    heads_local = query_cot.shape[1]
    token_total = input_act.shape[0] * lax.axis_size("fs") * lax.axis_size("rep")
    scale_tokens = 1.0 / math.sqrt(token_total)
    gradient = lax.psum_scatter(
        jnp.concatenate(
            [contract_rows(input_act, query_cot), contract_rows(out_cot, attn_out)], axis=1
        ).astype(jnp.bfloat16),
        "fs",
        scatter_dimension=0,
        tiled=True,
    ).astype(jnp.float32)
    partial_value = jnp.concatenate(
        [
            contract_exact(query_factor, gradient[:, :heads_local]),
            contract_exact(out_factor, gradient[:, heads_local:]),
        ],
        axis=1,
    )
    projected = lax.psum_scatter(
        partial_value.astype(jnp.bfloat16), "fs", scatter_dimension=0, tiled=True
    ).astype(jnp.float32)
    projected = lax.psum(projected.astype(jnp.bfloat16), "rep").astype(jnp.float32) * scale_tokens
    proj_q = projected[:, :heads_local]
    proj_o = projected[:, heads_local:]
    new_first_q = 0.8 * first_q + 0.2 * proj_q
    new_second_q = 0.9 * second_q + 0.1 * proj_q * proj_q
    new_first_o = 0.8 * first_o + 0.2 * proj_o
    new_second_o = 0.9 * second_o + 0.1 * proj_o * proj_o
    dir_q = new_first_q / jnp.sqrt(new_second_q)
    dir_o = new_first_o / jnp.sqrt(new_second_o)
    local_squares = jnp.sum(dir_q * dir_q) + jnp.sum(dir_o * dir_o)
    total_squares = lax.psum(local_squares, ("fs", "tp"))
    norm_scale = jnp.sqrt(total_squares / (2 * RANK * HQ) + 1e-06)
    whole_dir_q, whole_dir_o = (
        lax.all_gather(dir_q, "fs", axis=0, tiled=True),
        lax.all_gather(dir_o, "fs", axis=0, tiled=True),
    )
    query_step = exact_dot(query_factor.astype(jnp.float32), whole_dir_q) / norm_scale
    out_step = (exact_dot(out_factor.astype(jnp.float32), whole_dir_o) / norm_scale).T
    new_query_w = query_w - 0.01 * query_step
    new_out_w = out_w - 0.01 * out_step
    query_copy = lax.all_gather(new_query_w.astype(jnp.bfloat16), "fs", axis=0, tiled=True)
    out_copy = lax.all_gather(new_out_w.astype(jnp.bfloat16), "fs", axis=1, tiled=True)
    return (
        new_query_w,
        new_out_w,
        query_step,
        out_step,
        new_first_q,
        new_second_q,
        new_first_o,
        new_second_o,
        query_copy,
        out_copy,
    )


def solution(mesh):
    return jax.shard_map(
        body,
        mesh=mesh,
        in_specs=(
            P(("fs", "rep"), None),
            P(("fs", "rep"), "tp"),
            P(("fs", "rep"), None),
            P(("fs", "rep"), "tp"),
            P("fs", "tp"),
            P("tp", "fs"),
            P("fs", None),
            P("fs", None),
            P("fs", "tp"),
            P("fs", "tp"),
            P("fs", "tp"),
            P("fs", "tp"),
        ),
        out_specs=(
            P("fs", "tp"),
            P("tp", "fs"),
            P("fs", "tp"),
            P("tp", "fs"),
            P("fs", "tp"),
            P("fs", "tp"),
            P("fs", "tp"),
            P("fs", "tp"),
            P(None, "tp"),
            P("tp", None),
        ),
        check_vma=False,
    )
```

profile of v0, /device:TPU:0, one launch (start us, length us, event | category | flops | bytes accessed | tf_op | source)
XLA Modules:
  0.0 343.3 jit_solution(11248011831809214401)
XLA Ops:
  7.2 0.0 reduce-scatter.5.cloned.1.call-start
  7.2 1.8 copy-done
  9.1 3.1 convolution_convert_fusion.1
  12.2 1.9 convolution_convert_fusion
  14.1 2.5 pad_maximum_fusion
  16.7 0.0 reduce-scatter.5.cloned.1.call-update
  16.7 0.0 reduce-scatter.7.cloned.1.call-start
  16.8 79.6 %reduce-scatter.5.cloned.1.call-done = bf16[512,1024]{0,1:T(8,128)(2,1)} async-done(((bf16[2048,1024]{0,1:T(8,128)(2,1)}), bf16[512,1024]{0,1:T(8,128)(2,1)}) %reduce-scatter.5.cloned.1.call-update) | async-done | bytes 1048592 | tf_op jit(solution)/shard_map/reduce_scatter | solution.py:50
  96.4 1.6 fusion.2
  98.0 1.6 fusion.1
  99.7 1.0 pad_maximum_fusion.1
  100.7 2.3 copy.59
  103.0 0.0 reduce-scatter.7.cloned.1.call-update
  103.0 0.0 all-reduce.2.cloned.1.call-start
  103.0 27.9 %reduce-scatter.7.cloned.1.call-done = bf16[128,1024]{1,0:T(8,128)(2,1)} async-done(((bf16[512,1024]{1,0:T(8,128)(2,1)}), bf16[128,1024]{1,0:T(8,128)(2,1)}) %reduce-scatter.7.cloned.1.call-update) | async-done | bytes 262160
  130.9 1.8 copy.60
  132.7 0.0 all-reduce.2.cloned.1.call-update
  132.8 0.0 all-gather.5.cloned.1.call-start
  132.8 0.8 copy.40
  133.7 1.8 copy.41
  135.4 1.8 copy.42
  137.2 1.8 copy.43
  139.0 37.0 %all-reduce.2.cloned.1.call-done = bf16[128,1024]{0,1:T(8,128)(2,1)} async-done(((bf16[128,1024]{0,1:T(8,128)(2,1)}), bf16[128,1024]{0,1:T(8,128)(2,1)}) %all-reduce.2.cloned.1.call-update) | async-done | bytes 262160 | tf_op jit(solution)/shard_map/psum | solution.py:68
  176.0 1.0 convert_multiply_fusion
  177.0 2.9 multiply_reduce_fusion
  179.9 0.0 all-gather.7.cloned.1.call-start
  180.0 0.5 all-gather.7.cloned.1.call-update
  180.5 0.0 all-gather.9.cloned.1.call-start
  181.9 2.5 copy.45
  184.4 16.9 %psum.15 = f32[]{:T(128)} all-reduce(f32[]{:T(128)S(6)} %add.30), channel_id=1, replica_groups=mesh['fs'=4,'rep'=4,'tp'=2] {'fs','tp'}, use_global_device_ids=true, to_apply=%region_5.0 | all-reduce | flops 1 | bytes 8 | tf_op jit(solution)/shard_map/psum | solution.py:78
  202.0 8.3 %all-gather.5.cloned.1.call-done = f32[512,512]{0,1:T(8,128)} async-done(((f32[128,512]{0,1:T(8,128)}), f32[512,512]{0,1:T(8,128)}) %all-gather.5.cloned.1.call-update) | async-done | bytes 1048592 | tf_op jit(solution)/shard_map/all_gather | solution.py:81
  210.3 4.2 %fusion.8 = (bf16[512,512]{0,1:T(8,128)(2,1)}, f32[512,512]{0,1:T(8,128)}, f32[512,512]{0,1:T(8,128)}) fusion(f32[512,512]{0,1:T(8,128)} %copy.45, f32[]{:T(128)S(6)} %sqrt.11, f32[512,512]{0,1:T(8,128)} %all-gather.5.cloned.1.call-done, bf16[512,512]{1,0:T(8,128)(2,1)} %param.18), kind=kOutput, calls=%fused_computation.27 | convolution fusion | flops 1611661312 | bytes 5242884 | tf_op jit(solution)/shard_map/dot_general | solution.py:28
  214.6 0.0 all-gather.11.cloned.1.call-start
  214.6 2.5 copy.47
  217.1 23.4 %all-gather.7.cloned.1.call-done = f32[512,512]{0,1:T(8,128)} async-done(((f32[128,512]{0,1:T(8,128)}), f32[512,512]{0,1:T(8,128)}) %all-gather.7.cloned.1.call-update) | async-done | bytes 1048592 | tf_op jit(solution)/shard_map/all_gather | solution.py:82
  240.5 4.3 %fusion.7 = (bf16[512,512]{0,1:T(8,128)(2,1)}, f32[512,512]{0,1:T(8,128)}, f32[512,512]{0,1:T(8,128)}) fusion(f32[512,512]{0,1:T(8,128)} %copy.47, f32[]{:T(128)S(6)} %sqrt.11, f32[512,512]{0,1:T(8,128)} %all-gather.7.cloned.1.call-done, bf16[512,512]{1,0:T(8,128)(2,1)} %param.19), kind=kOutput, calls=%fused_computation.26 | convolution fusion | flops 1611661312 | bytes 5242884 | tf_op jit(solution)/shard_map/dot_general | solution.py:28
  244.9 1.8 copy.55
  246.6 1.8 copy.54
  248.4 1.8 copy.53
  250.2 0.8 copy.52
  251.1 2.5 copy.49
  253.6 2.5 copy.51
  256.1 2.5 copy.48
  258.7 2.5 copy.50
  261.2 25.3 %all-gather.9.cloned.1.call-done = bf16[2048,512]{0,1:T(8,128)(2,1)} async-done(((bf16[512,512]{0,1:T(8,128)(2,1)}), bf16[2048,512]{0,1:T(8,128)(2,1)}) %all-gather.9.cloned.1.call-update) | async-done | bytes 2097168 | tf_op jit(solution)/shard_map/all_gather | solution.py:88
  286.5 3.9 %copy.56 = bf16[2048,512]{1,0:T(8,128)(2,1)} copy(bf16[2048,512]{0,1:T(8,128)(2,1)} %all-gather.9.cloned.1.call-done) | data formatting | bytes 4194304
  290.4 42.1 %all-gather.11.cloned.1.call-done = bf16[512,2048]{0,1:T(8,128)(2,1)} async-done(((bf16[512,512]{0,1:T(8,128)(2,1)}), bf16[512,2048]{0,1:T(8,128)(2,1)}) %all-gather.11.cloned.1.call-update) | async-done | bytes 2097168 | tf_op jit(solution)/shard_map/all_gather | solution.py:89
  332.6 3.9 %copy.57 = bf16[512,2048]{1,0:T(8,128)(2,1)} copy(bf16[512,2048]{0,1:T(8,128)(2,1)} %all-gather.11.cloned.1.call-done) | data formatting | bytes 4194304
  (10 shorter events, 0.1 us)
Async XLA Ops:
  7.2 1.9 copy-start
  7.2 89.2 %reduce-scatter.5.cloned.1.call-start = ((), (), s32[]{:S(2)}) async-start(), calls=%async_computation.2 | async-start | bytes 5242880 | tf_op jit(solution)/shard_map/reduce_scatter | solution.py:50
  9.1 3.1 copy-start.2
  9.1 3.1 copy-start.3
  16.7 114.2 %reduce-scatter.7.cloned.1.call-start = ((), (), s32[]{:S(2)}) async-start(), calls=%async_computation.8 | async-start | bytes 1310720
  99.7 33.2 %copy-start.1 = (f32[128,512]{1,0:T(8,128)S(1)}, f32[128,512]{1,0:T(8,128)}, u32[]{:S(2)}) copy-start(f32[128,512]{1,0:T(8,128)} %param.20) | copy-start | bytes 786436
  103.0 73.0 %all-reduce.2.cloned.1.call-start = ((), (), s32[]{:S(2)}) async-start(), calls=%async_computation.3 | async-start | bytes 524288 | tf_op jit(solution)/shard_map/psum | solution.py:68
  132.8 77.5 %all-gather.5.cloned.1.call-start = ((), (), s32[]{:S(2)}) async-start(), calls=%async_computation.4 | async-start | bytes 1310720 | tf_op jit(solution)/shard_map/all_gather | solution.py:81
  179.9 60.6 %all-gather.7.cloned.1.call-start = ((), (), s32[]{:S(2)}) async-start(), calls=%async_computation.5 | async-start | bytes 1310720 | tf_op jit(solution)/shard_map/all_gather | solution.py:82
  180.5 106.0 %all-gather.9.cloned.1.call-start = ((), (), s32[]{:S(2)}) async-start(), calls=%async_computation.6 | async-start | bytes 2621440 | tf_op jit(solution)/shard_map/all_gather | solution.py:88
  214.6 118.0 %all-gather.11.cloned.1.call-start = ((), (), s32[]{:S(2)}) async-start(), calls=%async_computation.7 | async-start | bytes 2621440 | tf_op jit(solution)/shard_map/all_gather | solution.py:89
Sparse Core Ops, SparseCore 0:
  16.8 79.5 reduce-scatter.4
  103.1 27.7 reduce-scatter.6
  134.4 41.5 all-reduce.1
  180.1 30.1 all-gather.4
  212.3 28.2 all-gather.6
  242.5 43.9 all-gather.8
  288.1 44.4 all-gather.10
where the time goes:
time: 344 us; the launch traced here: 343 us
  waiting for transfers between devices  244 us (71%)
  local copies, waits for them, and re-layouts  41.3 us (12%)
  blocking collectives  16.9 us (5%)
  matrix products  16.8 us (5%)
  between operations  16.2 us (5%)
  other arithmetic  7.46 us (2%)
    reduce_scatter x1, waiting for transfers between devices, body(): lax.psum_scatter(jnp.concatenate([contract_rows(input_act, query_cot), co...  79.6 us
    all_gather x1, waiting for transfers between devices, body(): lax.all_gather(new_out_w.astype(jnp.bfloat16), 'fs', axis=1, tiled=True)  42.1 us
    unnamed x26, local copies, waits for them, and re-layouts  41.3 us
    psum x1, waiting for transfers between devices, body(): lax.psum(projected.astype(jnp.bfloat16), 'rep').astype(jnp.float32)  37 us
    unnamed x8, waiting for transfers between devices  28.5 us
    all_gather x1, waiting for transfers between devices, body(): lax.all_gather(new_query_w.astype(jnp.bfloat16), 'fs', axis=0, tiled=True)  25.3 us
    all_gather x1, waiting for transfers between devices, body(): lax.all_gather(dir_o, 'fs', axis=0, tiled=True)  23.4 us
    psum x1, blocking collectives, body(): total_squares = lax.psum(local_squares, ('fs', 'tp'))  16.9 us
  transfers between devices with their start and end apart: 7, of which 7 were waited for; matrix products, arithmetic and copies ran while one was open for 12% of the time, Pallas kernels for 0%

commit v1 on v0

--- a/solution.py
+++ b/solution.py
@@ -85,7 +85,12 @@
     out_step = (exact_dot(out_factor.astype(jnp.float32), whole_dir_o) / norm_scale).T
     new_query_w = query_w - 0.01 * query_step
     new_out_w = out_w - 0.01 * out_step
-    query_copy = lax.all_gather(new_query_w.astype(jnp.bfloat16), "fs", axis=0, tiled=True)
+    query_copy = jnp.concatenate(
+        lax.all_to_all(
+            jnp.stack([new_query_w.astype(jnp.bfloat16)] * lax.axis_size("fs")), "fs", 0, 0
+        ),
+        axis=0,
+    )
     out_copy = lax.all_gather(new_out_w.astype(jnp.bfloat16), "fs", axis=1, tiled=True)
     return (
         new_query_w,

time: 344 us -> 340 us (0.988)
  waiting for transfers between devices: 244 us -> 232 us
  starting transfers between devices: 0.29 us -> 4.7 us
  local copies, waits for them, and re-layouts: 41.3 us -> 45 us
    all_gather x1 -> x0, waiting for transfers between devices: 25.3 us -> none  [body(): lax.all_gather(new_query_w.astype(jnp.bfloat16), 'fs', axis=0, tiled=True)]
    all_gather x1, waiting for transfers between devices: 23.4 us -> 35.9 us  [body(): lax.all_gather(dir_o, 'fs', axis=0, tiled=True)]
    all_to_all x0 -> x1, waiting for transfers between devices: none -> 4.56 us  [body(): lax.all_to_all(jnp.stack([new_query_w.astype(jnp.bfloat16)] * lax.axis_si...]
    all_to_all x0 -> x1, starting transfers between devices: none -> 4.45 us  [body(): lax.all_to_all(jnp.stack([new_query_w.astype(jnp.bfloat16)] * lax.axis_si...]
    unnamed x8 -> x7, waiting for transfers between devices: 28.5 us -> 28.5 us
where the time goes in v1:
time: 340 us; the launch traced here: 339 us
  waiting for transfers between devices  232 us (68%)
  local copies, waits for them, and re-layouts  45 us (13%)
  blocking collectives  17 us (5%)
  matrix products  16.9 us (5%)
  between operations  16.2 us (5%)
  other arithmetic  7.5 us (2%)
  starting transfers between devices  4.7 us (1%)
    reduce_scatter x1, waiting for transfers between devices, body(): lax.psum_scatter(jnp.concatenate([contract_rows(input_act, query_cot), co...  79.6 us
    all_gather x1, waiting for transfers between devices, body(): lax.all_gather(new_out_w.astype(jnp.bfloat16), 'fs', axis=1, tiled=True)  40.5 us
    unnamed x26, local copies, waits for them, and re-layouts  40.4 us
    psum x1, waiting for transfers between devices, body(): lax.psum(projected.astype(jnp.bfloat16), 'rep').astype(jnp.float32)  37 us
    all_gather x1, waiting for transfers between devices, body(): lax.all_gather(dir_o, 'fs', axis=0, tiled=True)  35.9 us
    unnamed x7, waiting for transfers between devices  28.5 us
    psum x1, blocking collectives, body(): total_squares = lax.psum(local_squares, ('fs', 'tp'))  17 us
    dot_general x2, matrix products, exact_dot(): jnp.dot(left_side, right_side, precision=lax.Precision.HIGHEST, preferred...  8.55 us
  transfers between devices with their start and end apart: 7, of which 7 were waited for; matrix products, arithmetic and copies ran while one was open for 12% of the time, Pallas kernels for 0%

profile of v1, /device:TPU:0, one launch (start us, length us, event | category | flops | bytes accessed | tf_op | source)
XLA Modules:
  0.0 339.1 jit_solution(16285674474355395679)
XLA Ops:
  7.2 0.0 reduce-scatter.5.cloned.1.call-start
  7.2 1.8 copy-done
  9.1 3.1 convolution_convert_fusion
  12.2 1.9 convolution_convert_fusion.1
  14.1 2.5 pad_maximum_fusion
  16.7 0.0 reduce-scatter.7.cloned.1.call-start
  16.8 79.6 %reduce-scatter.5.cloned.1.call-done = bf16[512,1024]{0,1:T(8,128)(2,1)} async-done(((bf16[2048,1024]{0,1:T(8,128)(2,1)}), bf16[512,1024]{0,1:T(8,128)(2,1)}) %reduce-scatter.5.cloned.1.call-update) | async-done | bytes 1048592 | tf_op jit(solution)/shard_map/reduce_scatter | solution.py:50
  96.4 1.6 fusion.2
  98.0 1.6 fusion.1
  99.7 1.0 pad_maximum_fusion.1
  100.7 2.3 copy.59
  103.0 0.0 reduce-scatter.7.cloned.1.call-update
  103.0 0.0 all-reduce.2.cloned.1.call-start
  103.0 27.9 %reduce-scatter.7.cloned.1.call-done = bf16[128,1024]{1,0:T(8,128)(2,1)} async-done(((bf16[512,1024]{1,0:T(8,128)(2,1)}), bf16[128,1024]{1,0:T(8,128)(2,1)}) %reduce-scatter.7.cloned.1.call-update) | async-done | bytes 262160
  130.9 1.8 copy.60
  132.8 0.0 all-gather.4.cloned.1.call-start
  132.8 0.8 copy.43
  133.6 1.8 copy.42
  135.4 1.8 copy.41
  137.2 1.8 copy.40
  139.0 37.0 %all-reduce.2.cloned.1.call-done = bf16[128,1024]{0,1:T(8,128)(2,1)} async-done(((bf16[128,1024]{0,1:T(8,128)(2,1)}), bf16[128,1024]{0,1:T(8,128)(2,1)}) %all-reduce.2.cloned.1.call-update) | async-done | bytes 262160 | tf_op jit(solution)/shard_map/psum | solution.py:68
  176.0 1.0 convert_multiply_fusion
  177.0 2.9 multiply_reduce_fusion
  180.0 0.0 all-gather.6.cloned.1.call-start
  180.0 0.5 all-gather.6.cloned.1.call-update
  180.6 2.5 copy.45
  184.4 2.5 copy.47
  186.9 17.0 %psum.15 = f32[]{:T(128)} all-reduce(f32[]{:T(128)S(6)} %add.30), channel_id=1, replica_groups=mesh['fs'=4,'rep'=4,'tp'=2] {'fs','tp'}, use_global_device_ids=true, to_apply=%region_5.0 | all-reduce | flops 1 | bytes 8 | tf_op jit(solution)/shard_map/psum | solution.py:78
  204.6 5.7 %all-gather.4.cloned.1.call-done = f32[512,512]{0,1:T(8,128)} async-done(((f32[128,512]{0,1:T(8,128)}), f32[512,512]{0,1:T(8,128)}) %all-gather.4.cloned.1.call-update) | async-done | bytes 1048592 | tf_op jit(solution)/shard_map/all_gather | solution.py:81
  210.3 4.2 %fusion.8 = (bf16[512,512]{0,1:T(8,128)(2,1)}, f32[512,512]{0,1:T(8,128)}, f32[512,512]{0,1:T(8,128)}) fusion(f32[512,512]{0,1:T(8,128)} %copy.45, f32[]{:T(128)S(6)} %sqrt.11, f32[512,512]{0,1:T(8,128)} %all-gather.4.cloned.1.call-done, bf16[512,512]{1,0:T(8,128)(2,1)} %param.18), kind=kOutput, calls=%fused_computation.27 | convolution fusion | flops 1611661312 | bytes 5242884 | tf_op jit(solution)/shard_map/dot_general | solution.py:28
  214.6 2.0 copy.48
  216.6 2.5 stack.2
  219.1 4.5 %all-to-all-start = ((bf16[4,512,512]{2,1,0:T(8,128)(2,1)}), bf16[4,512,512]{2,1,0:T(8,128)(2,1)}, u32[]{:S(2)}, u32[]{:S(2)}) async-start(bf16[4,512,512]{2,1,0:T(8,128)(2,1)} %stack.2), calls=%async_computation.1 | async-start | bytes 4194304 | tf_op jit(solution)/shard_map/all_to_all | solution.py:89
  223.6 0.0 all-gather.8.cloned.1.call-start
  223.6 35.9 %all-gather.6.cloned.1.call-done = f32[512,512]{0,1:T(8,128)} async-done(((f32[128,512]{0,1:T(8,128)}), f32[512,512]{0,1:T(8,128)}) %all-gather.6.cloned.1.call-update) | async-done | bytes 1048592 | tf_op jit(solution)/shard_map/all_gather | solution.py:82
  259.6 4.3 %fusion.7 = (bf16[512,512]{0,1:T(8,128)(2,1)}, f32[512,512]{0,1:T(8,128)}, f32[512,512]{0,1:T(8,128)}) fusion(f32[512,512]{0,1:T(8,128)} %copy.47, f32[]{:T(128)S(6)} %sqrt.11, f32[512,512]{0,1:T(8,128)} %all-gather.6.cloned.1.call-done, bf16[512,512]{1,0:T(8,128)(2,1)} %param.19), kind=kOutput, calls=%fused_computation.26 | convolution fusion | flops 1611661312 | bytes 5242884 | tf_op jit(solution)/shard_map/dot_general | solution.py:28
  263.9 1.8 copy.53
  265.7 1.8 copy.54
  267.5 1.8 copy.55
  269.3 0.8 copy.56
  270.1 2.5 copy.49
  272.6 2.5 copy.50
  275.2 2.5 copy.51
  277.7 2.5 copy.52
  280.2 4.6 %all-to-all-done = bf16[4,512,512]{2,1,0:T(8,128)(2,1)} async-done(((bf16[4,512,512]{2,1,0:T(8,128)(2,1)}), bf16[4,512,512]{2,1,0:T(8,128)(2,1)}, u32[]{:S(2)}, u32[]{:S(2)}) %all-to-all-start) | async-done | bytes 2097184 | tf_op jit(solution)/shard_map/all_to_all | solution.py:89
  284.8 40.5 %all-gather.8.cloned.1.call-done = bf16[512,2048]{0,1:T(8,128)(2,1)} async-done(((bf16[512,512]{0,1:T(8,128)(2,1)}), bf16[512,2048]{0,1:T(8,128)(2,1)}) %all-gather.8.cloned.1.call-update) | async-done | bytes 2097168 | tf_op jit(solution)/shard_map/all_gather | solution.py:94
  325.3 3.9 %copy.57 = bf16[512,2048]{1,0:T(8,128)(2,1)} copy(bf16[512,2048]{0,1:T(8,128)(2,1)} %all-gather.8.cloned.1.call-done) | data formatting | bytes 4194304
  329.2 3.0 copy.63
  (11 shorter events, 0.1 us)
Async XLA Ops:
  7.2 1.9 copy-start
  7.2 89.2 %reduce-scatter.5.cloned.1.call-start = ((), (), s32[]{:S(2)}) async-start(), calls=%async_computation.3 | async-start | bytes 5242880 | tf_op jit(solution)/shard_map/reduce_scatter | solution.py:50
  9.1 3.1 copy-start.2
  9.1 3.1 copy-start.3
  16.7 114.2 %reduce-scatter.7.cloned.1.call-start = ((), (), s32[]{:S(2)}) async-start(), calls=%async_computation.8 | async-start | bytes 1310720
  99.7 33.2 %copy-start.1 = (f32[128,512]{1,0:T(8,128)S(1)}, f32[128,512]{1,0:T(8,128)}, u32[]{:S(2)}) copy-start(f32[128,512]{1,0:T(8,128)} %param.23) | copy-start | bytes 786436
  103.0 73.0 %all-reduce.2.cloned.1.call-start = ((), (), s32[]{:S(2)}) async-start(), calls=%async_computation.4 | async-start | bytes 524288 | tf_op jit(solution)/shard_map/psum | solution.py:68
  132.8 77.6 %all-gather.4.cloned.1.call-start = ((), (), s32[]{:S(2)}) async-start(), calls=%async_computation.5 | async-start | bytes 1310720 | tf_op jit(solution)/shard_map/all_gather | solution.py:81
  180.0 79.6 %all-gather.6.cloned.1.call-start = ((), (), s32[]{:S(2)}) async-start(), calls=%async_computation.6 | async-start | bytes 1310720 | tf_op jit(solution)/shard_map/all_gather | solution.py:82
  219.1 65.7 %all-to-all-start = ((bf16[4,512,512]{2,1,0:T(8,128)(2,1)}), bf16[4,512,512]{2,1,0:T(8,128)(2,1)}, u32[]{:S(2)}, u32[]{:S(2)}) async-start(bf16[4,512,512]{2,1,0:T(8,128)(2,1)} %stack.2), calls=%async_computation.1 | async-start | bytes 4194304 | tf_op jit(solution)/shard_map/all_to_all | solution.py:89
  223.6 101.7 %all-gather.8.cloned.1.call-start = ((), (), s32[]{:S(2)}) async-start(), calls=%async_computation.7 | async-start | bytes 2621440 | tf_op jit(solution)/shard_map/all_gather | solution.py:94
Sparse Core Ops, SparseCore 0:
  16.8 79.5 reduce-scatter.4
  103.1 27.7 reduce-scatter.6
  134.4 41.5 all-reduce.1
  180.1 30.1 all-gather.3
  212.3 47.2 all-gather.5
  264.0 61.2 all-gather.7
